TPU v7x, 32 devices: a whole 2x2x4 slice. The times are simulated.
32 devices in a mesh: fs: 8 (over z, x), tp: 4 (over y, core).
Axes of the slice: x: 2, y: 2, z: 4, core: 2. Of those that a mesh axis runs over, the one named last changes fastest.
Arguments:
- tokens: bfloat16 [4096, 2048], P(('fs', 'tp')), may hold values from -6 to 6
- gate_weight: bfloat16 [5632, 2048], P('tp', 'fs'), may hold values from -0.125 to 0.125
- up_weight: bfloat16 [5632, 2048], P('tp', 'fs'), may hold values from -0.125 to 0.125
- down_weight: bfloat16 [5632, 2048], P('tp', 'fs'), may hold values from -0.078125 to 0.078125
- out_grad: bfloat16 [4096, 2048], P(('fs', 'tp')), may hold values from -6 to 6
Outputs:
- grad_tokens: bfloat16 [4096, 2048], P(('fs', 'tp'))
- grad_gate: float32 [5632, 2048], P('tp', 'fs')
- grad_up: float32 [5632, 2048], P('tp', 'fs')
- grad_down: float32 [5632, 2048], P('tp', 'fs')
- gate_rows: float32 [5632], P('tp')
- up_rows: float32 [5632], P('tp')
- down_rows: float32 [5632], P('tp')
All inputs are finite; a program needn't handle non-finite values.
Results may differ from a plain program's by a relative error of at most 0.014.
Values may be sent and summed in bfloat16 or wider, within the bound.
A program may use at most 128 MiB of HBM per device.

v0:
```python
import math
import jax
import jax.numpy as jnp
from jax import lax
from jax.sharding import PartitionSpec as P


def body(tokens, gate_weight, up_weight, down_weight, out_grad):
    inputs, cotangent = (
        lax.all_gather(tokens, "tp", axis=0, tiled=True),
        lax.all_gather(out_grad, "tp", axis=0, tiled=True),
    )
    w_gate, w_up, w_down = (
        lax.all_gather(gate_weight, "fs", axis=1, tiled=True),
        lax.all_gather(up_weight, "fs", axis=1, tiled=True),
        lax.all_gather(down_weight, "fs", axis=1, tiled=True),
    )
    inner = (((1,), (1,)), ((), ()))
    gate = lax.dot_general(inputs, w_gate, inner, preferred_element_type=jnp.float32)
    up = lax.dot_general(inputs, w_up, inner, preferred_element_type=jnp.float32)
    dhidden = lax.dot_general(cotangent, w_down, inner, preferred_element_type=jnp.float32)
    sig = jax.nn.sigmoid(gate)
    silu = gate * sig
    act = (silu * up).astype(jnp.bfloat16)
    dgate = (dhidden * up * sig * (1.0 + gate * (1.0 - sig))).astype(jnp.bfloat16)
    dup = (dhidden * silu).astype(jnp.bfloat16)
    term = jnp.dot(dgate, w_gate, preferred_element_type=jnp.float32)
    grad_tokens = lax.psum_scatter(
        (term + jnp.dot(dup, w_up, preferred_element_type=jnp.float32)).astype(jnp.bfloat16),
        "tp",
        scatter_dimension=0,
        tiled=True,
    )
    factor = 1.0 / math.sqrt(inputs.shape[0] * lax.axis_size("fs"))
    outer = (((0,), (0,)), ((), ()))
    width = gate_weight.shape[1] * lax.axis_size("fs")
    part_gate = lax.dot_general(dgate, inputs, outer, preferred_element_type=jnp.float32) * factor
    part_up = lax.dot_general(dup, inputs, outer, preferred_element_type=jnp.float32) * factor
    part_down = lax.dot_general(act, cotangent, outer, preferred_element_type=jnp.float32) * factor
    grad_gate, grad_up, grad_down = (
        lax.psum_scatter(
            part_gate.astype(jnp.bfloat16), "fs", scatter_dimension=1, tiled=True
        ).astype(jnp.float32),
        lax.psum_scatter(
            part_up.astype(jnp.bfloat16), "fs", scatter_dimension=1, tiled=True
        ).astype(jnp.float32),
        lax.psum_scatter(
            part_down.astype(jnp.bfloat16), "fs", scatter_dimension=1, tiled=True
        ).astype(jnp.float32),
    )
    sums = lax.psum(
        (
            jnp.sum(grad_gate * grad_gate, axis=1),
            jnp.sum(grad_up * grad_up, axis=1),
            jnp.sum(grad_down * grad_down, axis=1),
        ),
        "fs",
    )
    gate_rows, up_rows, down_rows = (sums[0] / width, sums[1] / width, sums[2] / width)
    return (grad_tokens, grad_gate, grad_up, grad_down, gate_rows, up_rows, down_rows)


def solution(mesh):
    return jax.shard_map(
        body,
        mesh=mesh,
        in_specs=(
            P(("fs", "tp"), None),
            P("tp", "fs"),
            P("tp", "fs"),
            P("tp", "fs"),
            P(("fs", "tp"), None),
        ),
        out_specs=(
            P(("fs", "tp"), None),
            P("tp", "fs"),
            P("tp", "fs"),
            P("tp", "fs"),
            P("tp"),
            P("tp"),
            P("tp"),
        ),
        check_vma=False,
    )
```

profile of v0, /device:TPU:0, one launch (start us, length us, event | category | flops | bytes accessed | tf_op | source)
XLA Modules:
  0.0 727.2 jit_solution(359217630501200977)
XLA Ops:
  7.2 0.0 all-gather.10.cloned.1.call-start
  7.2 0.7 all-gather.10.cloned.1.call-update
  7.9 0.0 all-gather.12.cloned.1.call-start
  7.9 0.7 all-gather.12.cloned.1.call-update
  8.6 0.0 all-gather.14.cloned.1.call-start
  8.7 0.7 all-gather.14.cloned.1.call-update
  9.4 0.0 all-gather.6.cloned.1.call-start
  9.4 0.5 all-gather.6.cloned.1.call-update
  10.0 0.0 all-gather.8.cloned.1.call-start
  10.0 0.5 all-gather.8.cloned.1.call-update
  10.5 0.0 reduce-scatter.11.cloned.1.call-start
  10.6 24.3 %all-gather.10.cloned.1.call-done = bf16[512,2048]{1,0:T(8,128)(2,1)} async-done(((bf16[128,2048]{1,0:T(8,128)(2,1)}), bf16[512,2048]{1,0:T(8,128)(2,1)}) %all-gather.10.cloned.1.call-update) | async-done | bytes 2097168 | tf_op jit(solution)/shard_map/all_gather | solution.py:10
  34.9 0.0 copy-start
  34.9 95.2 %all-gather.12.cloned.1.call-done = bf16[1408,2048]{1,0:T(8,128)(2,1)} async-done(((bf16[1408,256]{1,0:T(8,128)(2,1)}), bf16[1408,2048]{1,0:T(8,128)(2,1)}) %all-gather.12.cloned.1.call-update) | async-done | bytes 5767184 | tf_op jit(solution)/shard_map/all_gather | solution.py:15
  130.1 8.3 %fusion.3 = f32[512,1408]{1,0:T(8,128)} fusion(bf16[512,2048]{1,0:T(8,128)(2,1)} %all-gather.10.cloned.1.call-done, bf16[1408,2048]{1,0:T(8,128)(2,1)} %all-gather.12.cloned.1.call-done), kind=kOutput, calls=%fused_computation.16 | convolution fusion | flops 2952790016 | bytes 10747904 | tf_op jit(solution)/shard_map/dot_general | solution.py:20
  138.4 85.1 %all-gather.14.cloned.1.call-done = bf16[1408,2048]{1,0:T(8,128)(2,1)} async-done(((bf16[1408,256]{1,0:T(8,128)(2,1)}), bf16[1408,2048]{1,0:T(8,128)(2,1)}) %all-gather.14.cloned.1.call-update) | async-done | bytes 5767184 | tf_op jit(solution)/shard_map/all_gather | solution.py:14
  223.5 0.0 copy-done
  223.5 7.6 %fusion.4 = f32[512,1408]{1,0:T(8,128)} fusion(bf16[512,2048]{1,0:T(8,128)(2,1)S(1)} %copy-done, bf16[1408,2048]{1,0:T(8,128)(2,1)} %all-gather.14.cloned.1.call-done), kind=kOutput, calls=%fused_computation.17 | convolution fusion | flops 2952790016 | bytes 10747904 | tf_op jit(solution)/shard_map/dot_general | solution.py:19
  231.1 14.6 %all-gather.6.cloned.1.call-done = bf16[512,2048]{1,0:T(8,128)(2,1)} async-done(((bf16[128,2048]{1,0:T(8,128)(2,1)}), bf16[512,2048]{1,0:T(8,128)(2,1)}) %all-gather.6.cloned.1.call-update) | async-done | bytes 2097168 | tf_op jit(solution)/shard_map/all_gather | solution.py:11
  245.7 9.1 %multiply_convert_fusion = bf16[1408,2048]{1,0:T(8,128)(2,1)} fusion(bf16[512,2048]{1,0:T(8,128)(2,1)} %all-gather.6.cloned.1.call-done, f32[512,1408]{1,0:T(8,128)} %fusion.3, f32[512,1408]{1,0:T(8,128)} %fusion.4), kind=kOutput, calls=%fused_computation | convolution fusion | flops 2962882560 | bytes 13631488 | tf_op jit(solution)/shard_map/dot_general | solution.py:39
  254.7 0.0 reduce-scatter.11.cloned.1.call-update
  254.7 0.2 reduce-scatter.9.cloned.1.call-start
  255.0 85.7 %all-gather.8.cloned.1.call-done = bf16[1408,2048]{1,0:T(8,128)(2,1)} async-done(((bf16[1408,256]{1,0:T(8,128)(2,1)}), bf16[1408,2048]{1,0:T(8,128)(2,1)}) %all-gather.8.cloned.1.call-update) | async-done | bytes 5767184 | tf_op jit(solution)/shard_map/all_gather | solution.py:16
  340.7 10.2 %multiply_convert_fusion.4 = (bf16[512,1408]{1,0:T(8,128)(2,1)S(1)}, bf16[512,1408]{1,0:T(8,128)(2,1)}) fusion(f32[512,1408]{1,0:T(8,128)} %fusion.4, f32[512,1408]{1,0:T(8,128)} %fusion.3, bf16[512,2048]{1,0:T(8,128)(2,1)} %all-gather.6.cloned.1.call-done, bf16[1408,2048]{1,0:T(8,128)(2,1)} %all-gather.8.cloned.1.call-done), kind=kOutput, calls=%fused_computation.5 | convolution fusion | flops 2962161664 | bytes 16515072 | tf_op jit(solution)/shard_map/dot_general | solution.py:21
  350.9 5.0 multiply_convert_fusion.1
  355.9 0.0 reduce-scatter.9.cloned.1.call-update
  355.9 0.0 reduce-scatter.7.cloned.1.call-start
  355.9 6.5 multiply_convert_fusion.2
  362.4 0.0 copy-start.1
  362.4 0.0 reduce-scatter.7.cloned.1.call-update
  362.4 0.0 reduce-scatter.5.cloned.1.call-start
  362.5 1.3 copy-done.1
  363.8 5.4 fusion.5
  369.2 7.4 %add_convert_fusion = bf16[512,2048]{1,0:T(8,128)(2,1)} fusion(f32[512,2048]{1,0:T(8,128)S(1)} %fusion.5, bf16[512,1408]{1,0:T(8,128)(2,1)S(1)} %get-tuple-element.16, bf16[1408,2048]{1,0:T(8,128)(2,1)} %all-gather.12.cloned.1.call-done), kind=kOutput, calls=%fused_computation.3 | convolution fusion | flops 2954887168 | bytes 13500416 | tf_op jit(solution)/shard_map/dot_general | solution.py:29
  376.6 0.0 reduce-scatter.5.cloned.1.call-update
  376.6 76.8 %reduce-scatter.11.cloned.1.call-done = bf16[1408,256]{1,0:T(8,128)(2,1)} async-done(((bf16[1408,2048]{1,0:T(8,128)(2,1)}), bf16[1408,256]{1,0:T(8,128)(2,1)}) %reduce-scatter.11.cloned.1.call-update) | async-done | bytes 720912 | tf_op jit(solution)/shard_map/reduce_scatter | solution.py:47
  453.5 2.3 multiply_reduce_fusion
  455.8 111.8 %reduce-scatter.9.cloned.1.call-done = bf16[1408,256]{1,0:T(8,128)(2,1)} async-done(((bf16[1408,2048]{1,0:T(8,128)(2,1)}), bf16[1408,256]{1,0:T(8,128)(2,1)}) %reduce-scatter.9.cloned.1.call-update) | async-done | bytes 720912 | tf_op jit(solution)/shard_map/reduce_scatter | solution.py:44
  567.6 2.3 multiply_reduce_fusion.1
  569.9 111.8 %reduce-scatter.7.cloned.1.call-done = bf16[1408,256]{1,0:T(8,128)(2,1)} async-done(((bf16[1408,2048]{1,0:T(8,128)(2,1)}), bf16[1408,256]{1,0:T(8,128)(2,1)}) %reduce-scatter.7.cloned.1.call-update) | async-done | bytes 720912 | tf_op jit(solution)/shard_map/reduce_scatter | solution.py:41
  681.7 2.3 multiply_reduce_fusion.2
  684.0 35.5 %all-reduce = (f32[1408]{0:T(1024)S(1)}, f32[1408]{0:T(1024)S(1)}, f32[1408]{0:T(1024)S(1)}) all-reduce(f32[1408]{0:T(1024)S(1)} %get-tuple-element.14, f32[1408]{0:T(1024)S(1)} %get-tuple-element.12, f32[1408]{0:T(1024)S(1)} %get-tuple-element.10), channel_id=1, replica_groups=mesh['fs'=8,'tp'=4] {'fs'}, use_global_device_ids=true, to_apply=%region_5.0 | all-reduce | flops 4224 | bytes 33792 | tf_op jit(solution)/shard_map/psum | solution.py:51
  719.5 0.6 broadcast_multiply_fusion.2
  720.1 0.6 broadcast_multiply_fusion
  720.7 0.0 reduce-scatter.5.cloned.1.call-done
Async XLA Ops:
  7.2 27.7 %all-gather.10.cloned.1.call-start = ((), (), s32[]{:S(2)}) async-start(), calls=%async_computation.6 | async-start | bytes 2621440 | tf_op jit(solution)/shard_map/all_gather | solution.py:10
  7.9 122.2 %all-gather.12.cloned.1.call-start = ((), (), s32[]{:S(2)}) async-start(), calls=%async_computation.7 | async-start | bytes 6488064 | tf_op jit(solution)/shard_map/all_gather | solution.py:15
  8.6 214.8 %all-gather.14.cloned.1.call-start = ((), (), s32[]{:S(2)}) async-start(), calls=%async_computation.8 | async-start | bytes 6488064 | tf_op jit(solution)/shard_map/all_gather | solution.py:14
  9.4 236.3 %all-gather.6.cloned.1.call-start = ((), (), s32[]{:S(2)}) async-start(), calls=%async_computation.4 | async-start | bytes 2621440 | tf_op jit(solution)/shard_map/all_gather | solution.py:11
  10.0 330.7 %all-gather.8.cloned.1.call-start = ((), (), s32[]{:S(2)}) async-start(), calls=%async_computation.5 | async-start | bytes 6488064 | tf_op jit(solution)/shard_map/all_gather | solution.py:16
  10.5 442.9 %reduce-scatter.11.cloned.1.call-start = ((), (), s32[]{:S(2)}) async-start(), calls=%async_computation.12 | async-start | bytes 6488064 | tf_op jit(solution)/shard_map/reduce_scatter | solution.py:47
  34.9 188.6 %copy-start = (bf16[512,2048]{1,0:T(8,128)(2,1)S(1)}, bf16[512,2048]{1,0:T(8,128)(2,1)}, u32[]{:S(2)}) copy-start(bf16[512,2048]{1,0:T(8,128)(2,1)} %all-gather.10.cloned.1.call-done) | copy-start | bytes 6291460
  254.7 312.8 %reduce-scatter.9.cloned.1.call-start = ((), (), s32[]{:S(2)}) async-start(), calls=%async_computation.11 | async-start | bytes 6488064 | tf_op jit(solution)/shard_map/reduce_scatter | solution.py:44
  355.9 325.8 %reduce-scatter.7.cloned.1.call-start = ((), (), s32[]{:S(2)}) async-start(), calls=%async_computation.10 | async-start | bytes 6488064 | tf_op jit(solution)/shard_map/reduce_scatter | solution.py:41
  362.4 1.4 copy-start.1
  362.4 358.3 %reduce-scatter.5.cloned.1.call-start = ((), (), s32[]{:S(2)}) async-start(), calls=%async_computation.9 | async-start | bytes 2621440 | tf_op jit(solution)/shard_map/reduce_scatter | solution.py:28
Sparse Core Ops, SparseCore 0:
  9.5 25.2 all-gather.9
  36.9 93.1 all-gather.11
  132.1 91.3 all-gather.13
  224.9 20.7 all-gather.5
  247.5 93.1 all-gather.7
  344.2 109.1 reduce-scatter.10
  457.1 110.3 reduce-scatter.8
  571.2 110.3 reduce-scatter.6
  684.8 30.5 reduce-scatter.4
where the time goes:
time: 728 us; the launch traced here: 727 us
  waiting for transfers between devices  608 us (84%)
  matrix products  59.5 us (8%)
  blocking collectives  35.5 us (5%)
  between operations  13.9 us (2%)
  other arithmetic  8.24 us (1%)
    reduce_scatter x1, waiting for transfers between devices, body(): lax.psum_scatter(part_up.astype(jnp.bfloat16), 'fs', scatter_dimension=1,...  112 us
    reduce_scatter x1, waiting for transfers between devices, body(): lax.psum_scatter(part_gate.astype(jnp.bfloat16), 'fs', scatter_dimension=...  112 us
    all_gather x1, waiting for transfers between devices, body(): lax.all_gather(up_weight, 'fs', axis=1, tiled=True)  95.2 us
    all_gather x1, waiting for transfers between devices, body(): lax.all_gather(down_weight, 'fs', axis=1, tiled=True)  85.7 us
    all_gather x1, waiting for transfers between devices, body(): lax.all_gather(gate_weight, 'fs', axis=1, tiled=True)  85.1 us
    reduce_scatter x1, waiting for transfers between devices, body(): lax.psum_scatter(part_down.astype(jnp.bfloat16), 'fs', scatter_dimension=...  76.8 us
    psum x1, blocking collectives, body(): lax.psum((jnp.sum(grad_gate * grad_gate, axis=1), jnp.sum(grad_up * grad_...  35.5 us
    all_gather x1, waiting for transfers between devices, body(): lax.all_gather(tokens, 'tp', axis=0, tiled=True)  24.3 us
  transfers between devices with their start and end apart: 9, of which 8 were waited for; matrix products, arithmetic and copies ran while one was open for 9% of the time, Pallas kernels for 0%

commit v1 on v0

--- a/solution.py
+++ b/solution.py
@@ -3,6 +3,23 @@
 import jax.numpy as jnp
 from jax import lax
 from jax.sharding import PartitionSpec as P
+
+
+def in_order(tiles, dim):
+    shape = list(tiles.shape[1:])
+    shape[dim] *= tiles.shape[0]
+    return jnp.moveaxis(tiles, 0, dim).reshape(shape)
+
+
+def collect(value, axis, dim):
+    size = lax.axis_size(axis)
+    right = [(i, (i + 1) % size) for i in range(size)]
+    parts = [value]
+    while len(parts) < size:
+        parts.append(lax.ppermute(parts[-1], axis, right))
+    here = lax.axis_index(axis)
+    parts = jnp.stack(parts)[(here - jnp.arange(size)) % size]
+    return in_order(parts, dim)
 
 
 def body(tokens, gate_weight, up_weight, down_weight, out_grad):
@@ -13,7 +30,7 @@
     w_gate, w_up, w_down = (
         lax.all_gather(gate_weight, "fs", axis=1, tiled=True),
         lax.all_gather(up_weight, "fs", axis=1, tiled=True),
-        lax.all_gather(down_weight, "fs", axis=1, tiled=True),
+        collect(down_weight, "fs", 1),
     )
     inner = (((1,), (1,)), ((), ()))
     gate = lax.dot_general(inputs, w_gate, inner, preferred_element_type=jnp.float32)

time: 728 us -> 704 us (0.967)
  waiting for transfers between devices: 608 us -> 559 us
  local copies, waits for them, and re-layouts: 1.29 us -> 24.9 us
    ppermute x0 -> x7, waiting for transfers between devices: none -> 180 us  [collect(): parts.append(lax.ppermute(parts[-1], axis, right))]
    all_gather x1, waiting for transfers between devices: 95.2 us -> 0.01 us  [body(): lax.all_gather(up_weight, 'fs', axis=1, tiled=True)]
    all_gather x1 -> x0, waiting for transfers between devices: 85.7 us -> none  [body(): lax.all_gather(down_weight, 'fs', axis=1, tiled=True)]
    reduce_scatter x1, waiting for transfers between devices: 76.8 us -> 112 us  [body(): lax.psum_scatter(part_down.astype(jnp.bfloat16), 'fs', scatter_dimension=...]
    reduce_scatter x1, waiting for transfers between devices: 112 us -> 80.6 us  [body(): lax.psum_scatter(part_up.astype(jnp.bfloat16), 'fs', scatter_dimension=1,...]
    all_gather x1, waiting for transfers between devices: 85.1 us -> 58.9 us  [body(): lax.all_gather(gate_weight, 'fs', axis=1, tiled=True)]
    all_gather x1, waiting for transfers between devices: 24.3 us -> 0.01 us  [body(): lax.all_gather(tokens, 'tp', axis=0, tiled=True)]
    unnamed x4 -> x15, local copies, waits for them, and re-layouts: 1.29 us -> 9.64 us
  transfers between devices with their start and end apart: 9 -> 15, of which waited for: 8 -> 12; matrix products, arithmetic and copies ran while one was open for 9% -> 10% of each run, Pallas kernels for 0% -> 0%
where the time goes in v1:
time: 704 us
  waiting for transfers between devices  559 us (79%)
  matrix products  58.2 us (8%)
  blocking collectives  35.5 us (5%)
  local copies, waits for them, and re-layouts  24.9 us (4%)
  between operations  14.2 us (2%)
  other arithmetic  8.26 us (1%)
    ppermute x7, waiting for transfers between devices, collect(): parts.append(lax.ppermute(parts[-1], axis, right))  180 us
    reduce_scatter x1, waiting for transfers between devices, body(): lax.psum_scatter(part_down.astype(jnp.bfloat16), 'fs', scatter_dimension=...  112 us
    reduce_scatter x1, waiting for transfers between devices, body(): lax.psum_scatter(part_gate.astype(jnp.bfloat16), 'fs', scatter_dimension=...  112 us
    reduce_scatter x1, waiting for transfers between devices, body(): lax.psum_scatter(part_up.astype(jnp.bfloat16), 'fs', scatter_dimension=1,...  80.6 us
    all_gather x1, waiting for transfers between devices, body(): lax.all_gather(gate_weight, 'fs', axis=1, tiled=True)  58.9 us
    psum x1, blocking collectives, body(): lax.psum((jnp.sum(grad_gate * grad_gate, axis=1), jnp.sum(grad_up * grad_...  35.5 us
    all_gather x1, waiting for transfers between devices, body(): lax.all_gather(out_grad, 'tp', axis=0, tiled=True)  14.8 us
  transfers between devices with their start and end apart: 15, of which 12 were waited for; matrix products, arithmetic and copies ran while one was open for 10% of the time, Pallas kernels for 0%

profile of v1, /device:TPU:0, one launch (start us, length us, event | category | flops | bytes accessed | tf_op | source)
XLA Modules:
  0.0 703.8 jit_solution(16290445469296143164)
XLA Ops:
  7.2 0.0 copy-start
  7.2 0.0 all-gather.7.cloned.1.call-start
  7.2 0.7 all-gather.7.cloned.1.call-update
  7.9 0.0 all-gather.9.cloned.1.call-start
  8.0 0.7 all-gather.9.cloned.1.call-update
  8.7 0.0 all-gather.11.cloned.1.call-start
  8.7 0.7 all-gather.11.cloned.1.call-update
  9.4 0.0 all-gather.5.cloned.1.call-start
  9.4 3.0 collective-permute-start
  12.5 19.4 %collective-permute-done = bf16[1408,256]{1,0:T(8,128)(2,1)S(1)} collective-permute-done((bf16[1408,256]{1,0:T(8,128)(2,1)}, bf16[1408,256]{1,0:T(8,128)(2,1)S(1)}, u32[]{:S(2)}, u32[]{:S(2)}) %collective-permute-start) | collective-permute-done | bytes 720928 | tf_op jit(solution)/shard_map/ppermute | solution.py:19
  31.8 0.0 collective-permute-start.1
  31.8 21.9 %collective-permute-done.1 = bf16[1408,256]{1,0:T(8,128)(2,1)S(1)} collective-permute-done((bf16[1408,256]{1,0:T(8,128)(2,1)S(1)}, bf16[1408,256]{1,0:T(8,128)(2,1)S(1)}, u32[]{:S(2)}, u32[]{:S(2)}) %collective-permute-start.1) | collective-permute-done | bytes 720928 | tf_op jit(solution)/shard_map/ppermute | solution.py:19
  53.8 0.0 collective-permute-start.2
  53.8 0.0 all-gather.5.cloned.1.call-update
  53.8 0.0 reduce-scatter.9.cloned.1.call-start
  53.8 32.9 %collective-permute-done.2 = bf16[1408,256]{1,0:T(8,128)(2,1)S(1)} collective-permute-done((bf16[1408,256]{1,0:T(8,128)(2,1)S(1)}, bf16[1408,256]{1,0:T(8,128)(2,1)S(1)}, u32[]{:S(2)}, u32[]{:S(2)}) %collective-permute-start.2) | collective-permute-done | bytes 720928 | tf_op jit(solution)/shard_map/ppermute | solution.py:19
  86.8 0.0 collective-permute-start.3
  86.8 0.0 copy-done
  86.8 0.9 bitcast_dynamic-update-slice_fusion.7
  87.7 24.3 %collective-permute-done.3 = bf16[1408,256]{1,0:T(8,128)(2,1)S(1)} collective-permute-done((bf16[1408,256]{1,0:T(8,128)(2,1)S(1)}, bf16[1408,256]{1,0:T(8,128)(2,1)S(1)}, u32[]{:S(2)}, u32[]{:S(2)}) %collective-permute-start.3) | collective-permute-done | bytes 720928 | tf_op jit(solution)/shard_map/ppermute | solution.py:19
  112.1 0.0 collective-permute-start.4
  112.1 0.9 bitcast_dynamic-update-slice_fusion.6
  113.0 0.9 bitcast_dynamic-update-slice_fusion.5
  114.0 33.5 %collective-permute-done.4 = bf16[1408,256]{1,0:T(8,128)(2,1)S(1)} collective-permute-done((bf16[1408,256]{1,0:T(8,128)(2,1)S(1)}, bf16[1408,256]{1,0:T(8,128)(2,1)S(1)}, u32[]{:S(2)}, u32[]{:S(2)}) %collective-permute-start.4) | collective-permute-done | bytes 720928 | tf_op jit(solution)/shard_map/ppermute | solution.py:19
  147.4 0.0 collective-permute-start.5
  147.4 0.9 bitcast_dynamic-update-slice_fusion.4
  148.3 0.9 bitcast_dynamic-update-slice_fusion.3
  149.2 33.5 %collective-permute-done.5 = bf16[1408,256]{1,0:T(8,128)(2,1)S(1)} collective-permute-done((bf16[1408,256]{1,0:T(8,128)(2,1)S(1)}, bf16[1408,256]{1,0:T(8,128)(2,1)S(1)}, u32[]{:S(2)}, u32[]{:S(2)}) %collective-permute-start.5) | collective-permute-done | bytes 720928 | tf_op jit(solution)/shard_map/ppermute | solution.py:19
  182.8 0.0 collective-permute-start.6
  182.8 0.9 bitcast_dynamic-update-slice_fusion.2
  183.7 0.9 bitcast_dynamic-update-slice_fusion.1
  184.6 14.1 %collective-permute-done.6 = bf16[1408,256]{1,0:T(8,128)(2,1)S(1)} collective-permute-done((bf16[1408,256]{1,0:T(8,128)(2,1)S(1)}, bf16[1408,256]{1,0:T(8,128)(2,1)S(1)}, u32[]{:S(2)}, u32[]{:S(2)}) %collective-permute-start.6) | collective-permute-done | bytes 720928 | tf_op jit(solution)/shard_map/ppermute | solution.py:19
  198.7 0.9 bitcast_dynamic-update-slice_fusion
  199.7 6.1 gather_fusion
  205.7 8.3 %copy.22 = bf16[1408,8,256]{0,2,1:T(8,128)(2,1)} copy(bf16[1408,8,256]{2,0,1:T(8,128)(2,1)} %bitcast.37) | data formatting | bytes 11534336 | tf_op jit(solution)/shard_map/transpose | solution.py:11
  214.0 8.2 %fusion.5 = f32[512,1408]{0,1:T(8,128)} fusion(bf16[512,2048]{1,0:T(8,128)(2,1)} %all-gather.7.cloned.1.call-done, bf16[1408,2048]{1,0:T(8,128)(2,1)} %all-gather.9.cloned.1.call-done), kind=kOutput, calls=%fused_computation.33 | convolution fusion | flops 2952790016 | bytes 10747904 | tf_op jit(solution)/shard_map/dot_general | solution.py:37
  222.2 58.9 %all-gather.11.cloned.1.call-done = bf16[1408,2048]{1,0:T(8,128)(2,1)} async-done(((bf16[1408,256]{1,0:T(8,128)(2,1)}), bf16[1408,2048]{1,0:T(8,128)(2,1)}) %all-gather.11.cloned.1.call-update) | async-done | bytes 5767184 | tf_op jit(solution)/shard_map/all_gather | solution.py:31
  281.1 0.0 copy-done.1
  281.1 7.4 %fusion.6 = f32[512,1408]{0,1:T(8,128)} fusion(bf16[512,2048]{1,0:T(8,128)(2,1)S(1)} %copy-done.1, bf16[1408,2048]{1,0:T(8,128)(2,1)} %all-gather.11.cloned.1.call-done), kind=kOutput, calls=%fused_computation.34 | convolution fusion | flops 2952790016 | bytes 10747904 | tf_op jit(solution)/shard_map/dot_general | solution.py:36
  288.5 14.8 %all-gather.5.cloned.1.call-done = bf16[512,2048]{1,0:T(8,128)(2,1)} async-done(((bf16[128,2048]{1,0:T(8,128)(2,1)}), bf16[512,2048]{1,0:T(8,128)(2,1)}) %all-gather.5.cloned.1.call-update) | async-done | bytes 2097168 | tf_op jit(solution)/shard_map/all_gather | solution.py:28
  303.3 10.4 %multiply_convert_fusion.4 = (bf16[512,1408]{0,1:T(8,128)(2,1)S(1)}, bf16[512,1408]{0,1:T(8,128)(2,1)}) fusion(f32[512,1408]{0,1:T(8,128)} %fusion.6, f32[512,1408]{0,1:T(8,128)} %fusion.5, bf16[1408,2048]{0,1:T(8,128)(2,1)} %bitcast.38, bf16[512,2048]{1,0:T(8,128)(2,1)} %all-gather.5.cloned.1.call-done), kind=kOutput, calls=%fused_computation.7 | convolution fusion | flops 2962161664 | bytes 16515072 | tf_op jit(solution)/shard_map/dot_general | solution.py:38
  313.7 5.0 multiply_convert_fusion.1
  318.7 0.0 reduce-scatter.9.cloned.1.call-update
  318.7 0.0 reduce-scatter.7.cloned.1.call-start
  318.8 6.5 multiply_convert_fusion.2
  325.3 0.0 reduce-scatter.7.cloned.1.call-update
  325.3 0.0 reduce-scatter.11.cloned.1.call-start
  325.4 1.9 copy-done.2
  327.3 7.9 %multiply_convert_fusion = bf16[1408,2048]{1,0:T(8,128)(2,1)} fusion(bf16[512,2048]{1,0:T(8,128)(2,1)S(1)} %copy-done.2, f32[512,1408]{0,1:T(8,128)} %fusion.5, f32[512,1408]{0,1:T(8,128)} %fusion.6), kind=kOutput, calls=%fused_computation.1 | convolution fusion | flops 2962882560 | bytes 13631488 | tf_op jit(solution)/shard_map/dot_general | solution.py:56
  335.2 0.0 reduce-scatter.11.cloned.1.call-update
  335.2 0.0 reduce-scatter.5.cloned.1.call-start
  335.2 1.3 copy-done.3
  336.5 5.5 fusion.7
  342.0 7.4 %add_convert_fusion = bf16[512,2048]{1,0:T(8,128)(2,1)} fusion(f32[512,2048]{1,0:T(8,128)S(1)} %fusion.7, bf16[512,1408]{0,1:T(8,128)(2,1)S(1)} %get-tuple-element.16, bf16[1408,2048]{1,0:T(8,128)(2,1)} %all-gather.9.cloned.1.call-done), kind=kOutput, calls=%fused_computation.4 | convolution fusion | flops 2954887168 | bytes 13500416 | tf_op jit(solution)/shard_map/dot_general | solution.py:46
  349.4 0.0 reduce-scatter.5.cloned.1.call-update
  349.4 80.6 %reduce-scatter.9.cloned.1.call-done = bf16[1408,256]{1,0:T(8,128)(2,1)} async-done(((bf16[1408,2048]{1,0:T(8,128)(2,1)}), bf16[1408,256]{1,0:T(8,128)(2,1)}) %reduce-scatter.9.cloned.1.call-update) | async-done | bytes 720912 | tf_op jit(solution)/shard_map/reduce_scatter | solution.py:61
  429.9 2.3 multiply_reduce_fusion.1
  432.3 111.6 %reduce-scatter.7.cloned.1.call-done = bf16[1408,256]{1,0:T(8,128)(2,1)} async-done(((bf16[1408,2048]{1,0:T(8,128)(2,1)}), bf16[1408,256]{1,0:T(8,128)(2,1)}) %reduce-scatter.7.cloned.1.call-update) | async-done | bytes 720912 | tf_op jit(solution)/shard_map/reduce_scatter | solution.py:58
  543.8 2.3 multiply_reduce_fusion.2
  546.2 111.7 %reduce-scatter.11.cloned.1.call-done = bf16[1408,256]{1,0:T(8,128)(2,1)} async-done(((bf16[1408,2048]{1,0:T(8,128)(2,1)}), bf16[1408,256]{1,0:T(8,128)(2,1)}) %reduce-scatter.11.cloned.1.call-update) | async-done | bytes 720912 | tf_op jit(solution)/shard_map/reduce_scatter | solution.py:64
  657.9 2.3 multiply_reduce_fusion
  660.2 35.5 %all-reduce = (f32[1408]{0:T(1024)S(1)}, f32[1408]{0:T(1024)S(1)}, f32[1408]{0:T(1024)S(1)}) all-reduce(f32[1408]{0:T(1024)S(1)} %get-tuple-element.14, f32[1408]{0:T(1024)S(1)} %get-tuple-element.12, f32[1408]{0:T(1024)S(1)} %get-tuple-element.10), channel_id=1, replica_groups=mesh['fs'=8,'tp'=4] {'fs'}, use_global_device_ids=true, to_apply=%region_5.6 | all-reduce | flops 4224 | bytes 33792 | tf_op jit(solution)/shard_map/psum | solution.py:68
  695.7 0.6 broadcast_multiply_fusion.2
  696.3 0.6 broadcast_multiply_fusion
  (8 shorter events, 0.0 us)
Async XLA Ops:
  7.2 79.6 %copy-start = (bf16[1408,256]{1,0:T(8,128)(2,1)S(1)}, bf16[1408,256]{1,0:T(8,128)(2,1)}, u32[]{:S(2)}) copy-start(bf16[1408,256]{1,0:T(8,128)(2,1)} %param.8) | copy-start | bytes 2162692
  7.2 206.8 %all-gather.7.cloned.1.call-start = ((), (), s32[]{:S(2)}) async-start(), calls=%async_computation.5 | async-start | bytes 2621440 | tf_op jit(solution)/shard_map/all_gather | solution.py:27
  7.9 206.1 %all-gather.9.cloned.1.call-start = ((), (), s32[]{:S(2)}) async-start(), calls=%async_computation.6 | async-start | bytes 6488064 | tf_op jit(solution)/shard_map/all_gather | solution.py:32
  8.7 272.4 %all-gather.11.cloned.1.call-start = ((), (), s32[]{:S(2)}) async-start(), calls=%async_computation.7 | async-start | bytes 6488064 | tf_op jit(solution)/shard_map/all_gather | solution.py:31
  9.4 293.9 %all-gather.5.cloned.1.call-start = ((), (), s32[]{:S(2)}) async-start(), calls=%async_computation.4 | async-start | bytes 2621440 | tf_op jit(solution)/shard_map/all_gather | solution.py:28
  9.4 22.4 %collective-permute-start = (bf16[1408,256]{1,0:T(8,128)(2,1)}, bf16[1408,256]{1,0:T(8,128)(2,1)S(1)}, u32[]{:S(2)}, u32[]{:S(2)}) collective-permute-start(bf16[1408,256]{1,0:T(8,128)(2,1)} %param.8), channel_id=1, source_target_pairs={{0,4},{4,8},{8,12},{12,16},{16,20},{20,24},{24,28},{28,0},{1,5},{5... | collective-permute-start | bytes 2162696 | tf_op jit(solution)/shard_map/ppermute | solution.py:19
  31.8 21.9 %collective-permute-start.1 = (bf16[1408,256]{1,0:T(8,128)(2,1)S(1)}, bf16[1408,256]{1,0:T(8,128)(2,1)S(1)}, u32[]{:S(2)}, u32[]{:S(2)}) collective-permute-start(bf16[1408,256]{1,0:T(8,128)(2,1)S(1)} %collective-permute-done), channel_id=1, source_target_pairs={{0,4},{4,8},{8,12},{12,16},{16,20},{20,24},{24,28},{28,0},{1,5},{5... | collective-permute-start | bytes 2162696 | tf_op jit(solution)/shard_map/ppermute | solution.py:19
  53.8 33.0 %collective-permute-start.2 = (bf16[1408,256]{1,0:T(8,128)(2,1)S(1)}, bf16[1408,256]{1,0:T(8,128)(2,1)S(1)}, u32[]{:S(2)}, u32[]{:S(2)}) collective-permute-start(bf16[1408,256]{1,0:T(8,128)(2,1)S(1)} %collective-permute-done.1), channel_id=1, source_target_pairs={{0,4},{4,8},{8,12},{12,16},{16,20},{20,24},{24,28},{28,0},{1,5},{5... | collective-permute-start | bytes 2162696 | tf_op jit(solution)/shard_map/ppermute | solution.py:19
  53.8 376.2 %reduce-scatter.9.cloned.1.call-start = ((), (), s32[]{:S(2)}) async-start(), calls=%async_computation.10 | async-start | bytes 6488064 | tf_op jit(solution)/shard_map/reduce_scatter | solution.py:61
  86.8 25.3 %collective-permute-start.3 = (bf16[1408,256]{1,0:T(8,128)(2,1)S(1)}, bf16[1408,256]{1,0:T(8,128)(2,1)S(1)}, u32[]{:S(2)}, u32[]{:S(2)}) collective-permute-start(bf16[1408,256]{1,0:T(8,128)(2,1)S(1)} %collective-permute-done.2), channel_id=1, source_target_pairs={{0,4},{4,8},{8,12},{12,16},{16,20},{20,24},{24,28},{28,0},{1,5},{5... | collective-permute-start | bytes 2162696 | tf_op jit(solution)/shard_map/ppermute | solution.py:19
  112.1 35.4 %collective-permute-start.4 = (bf16[1408,256]{1,0:T(8,128)(2,1)S(1)}, bf16[1408,256]{1,0:T(8,128)(2,1)S(1)}, u32[]{:S(2)}, u32[]{:S(2)}) collective-permute-start(bf16[1408,256]{1,0:T(8,128)(2,1)S(1)} %collective-permute-done.3), channel_id=1, source_target_pairs={{0,4},{4,8},{8,12},{12,16},{16,20},{20,24},{24,28},{28,0},{1,5},{5... | collective-permute-start | bytes 2162696 | tf_op jit(solution)/shard_map/ppermute | solution.py:19
  147.4 35.4 %collective-permute-start.5 = (bf16[1408,256]{1,0:T(8,128)(2,1)S(1)}, bf16[1408,256]{1,0:T(8,128)(2,1)S(1)}, u32[]{:S(2)}, u32[]{:S(2)}) collective-permute-start(bf16[1408,256]{1,0:T(8,128)(2,1)S(1)} %collective-permute-done.4), channel_id=1, source_target_pairs={{0,4},{4,8},{8,12},{12,16},{16,20},{20,24},{24,28},{28,0},{1,5},{5... | collective-permute-start | bytes 2162696 | tf_op jit(solution)/shard_map/ppermute | solution.py:19
  182.8 15.9 %collective-permute-start.6 = (bf16[1408,256]{1,0:T(8,128)(2,1)S(1)}, bf16[1408,256]{1,0:T(8,128)(2,1)S(1)}, u32[]{:S(2)}, u32[]{:S(2)}) collective-permute-start(bf16[1408,256]{1,0:T(8,128)(2,1)S(1)} %collective-permute-done.5), channel_id=1, source_target_pairs={{0,4},{4,8},{8,12},{12,16},{16,20},{20,24},{24,28},{28,0},{1,5},{5... | collective-permute-start | bytes 2162696 | tf_op jit(solution)/shard_map/ppermute | solution.py:19
  214.0 67.1 %copy-start.1 = (bf16[512,2048]{1,0:T(8,128)(2,1)S(1)}, bf16[512,2048]{1,0:T(8,128)(2,1)}, u32[]{:S(2)}) copy-start(bf16[512,2048]{1,0:T(8,128)(2,1)} %all-gather.7.cloned.1.call-done) | copy-start | bytes 6291460
  318.7 225.1 %reduce-scatter.7.cloned.1.call-start = ((), (), s32[]{:S(2)}) async-start(), calls=%async_computation.9 | async-start | bytes 6488064 | tf_op jit(solution)/shard_map/reduce_scatter | solution.py:58
  325.3 2.0 copy-start.2
  325.3 332.6 %reduce-scatter.11.cloned.1.call-start = ((), (), s32[]{:S(2)}) async-start(), calls=%async_computation.11 | async-start | bytes 6488064 | tf_op jit(solution)/shard_map/reduce_scatter | solution.py:64
  335.2 1.4 copy-start.3
  335.2 361.7 %reduce-scatter.5.cloned.1.call-start = ((), (), s32[]{:S(2)}) async-start(), calls=%async_computation.8 | async-start | bytes 2621440 | tf_op jit(solution)/shard_map/reduce_scatter | solution.py:45
Sparse Core Ops, SparseCore 0:
  9.5 25.2 all-gather.6
  36.9 137.1 all-gather.8
  176.1 104.9 all-gather.10
  282.5 20.7 all-gather.4
  318.9 111.0 reduce-scatter.8
  433.5 110.3 reduce-scatter.6
  547.5 110.3 reduce-scatter.10
  661.0 30.4 reduce-scatter.4
